TPU v7x, 32 devices: a whole 2x2x4 slice. The times are simulated.
32 devices in a mesh: ep: 4 (over y, x), tp: 8 (over z, core).
Axes of the slice: x: 2, y: 2, z: 4, core: 2. Of those that a mesh axis runs over, the one named last changes fastest.
Arguments:
- residual: bfloat16 [128, 2048], P('ep'), may hold values from -20 to 20
- cache_latent: bfloat16 [128, 2048, 256], P(('ep', 'tp')), may hold values from -12 to 12
- cache_rope: bfloat16 [128, 32, 2048], P(('ep', 'tp')), may hold values from -6 to 6
- lengths: int32 [128], P(('ep', 'tp')), may hold values from 2 to 2048, as said below
- query_latent: bfloat16 [128, 32, 256], P(('ep', 'tp')), may hold values from -250 to 250
- query_rope: bfloat16 [128, 32, 32], P(('ep', 'tp')), may hold values from -6 to 6
- norm_gain: bfloat16 [2048], replicated, may hold values from 0.099609375 to 1.8984375
- latent_weight: bfloat16 [2048, 256], replicated, may hold values from -0.125 to 0.125
- latent_gain: bfloat16 [256], replicated, may hold values from 0.099609375 to 1.8984375
- rope_weight: bfloat16 [32, 2048], replicated, may hold values from -0.125 to 0.125
- value_weight: bfloat16 [256, 2048], replicated, may hold values from -0.375 to 0.375
- out_weight: bfloat16 [2048, 2048], P('tp'), may hold values from -1 to 1
- mixer_gain: bfloat16 [2048], replicated, may hold values from 0.099609375 to 1.8984375
- group_router: bfloat16 [2048, 4], replicated, may hold values from -0.0625 to 0.0625
- expert_router: bfloat16 [2048, 8], replicated, may hold values from -0.0625 to 0.0625
- expert_ids: int32 [128, 2], P('ep'), may hold values from 0 to 7, as said below
- gate_weight: bfloat16 [8, 2048, 4096], P('ep', None, 'tp'), may hold values from -0.125 to 0.125
- up_weight: bfloat16 [8, 2048, 4096], P('ep', None, 'tp'), may hold values from -0.125 to 0.125
- down_weight: bfloat16 [8, 4096, 2048], P('ep', 'tp'), may hold values from -0.75 to 0.75
Outputs:
- mixed: bfloat16 [128, 2048], P('ep')
- new_latent: bfloat16 [128, 256], P(('ep', 'tp'))
- new_rope_key: bfloat16 [128, 32], P(('ep', 'tp'))
Inputs may be any that keep to these rules, and one draw needn't show every extreme that they name: `lengths`: every sequence has 2 or more cached positions, and in every draw some sequence has all 2048. `expert_ids`: each row names 2 different experts of one group; group g holds experts g * 2 to g * 2 + 1. Among the rows of one index of ep (aligned blocks of 32 rows) no expert is named more than 16 times, and in every draw some expert is named exactly 16 times in every block.
All inputs are finite; a program needn't handle non-finite values.
Results may differ from a plain program's by a relative error of at most 0.012.
Values may be sent and summed in bfloat16 or wider, within the bound.
A program may use at most 64 MiB of HBM per device.

v0:
```python
import jax
import jax.numpy as jnp
from jax import lax
from jax.sharding import PartitionSpec as P

H = 32
KV = 256
ROPE = 32
NOPE = 64
V = 64
GROUPS = 4
TOPK = 2
NORM_EPSILON = 1e-06
ROPE_BASE = 10000.0


def inverse_rms(values):
    return lax.rsqrt(jnp.mean(values * values, axis=-1, keepdims=True) + NORM_EPSILON)


def rotate(vector, position):
    half_width = vector.shape[-1] // 2
    frequency = ROPE_BASE ** (
        -jnp.arange(0, vector.shape[-1], 2, dtype=jnp.float32) / vector.shape[-1]
    )
    angles = position[..., None] * frequency
    lower_half = vector[..., :half_width]
    upper_half = vector[..., half_width:]
    return jnp.concatenate(
        [
            lower_half * jnp.cos(angles) - upper_half * jnp.sin(angles),
            upper_half * jnp.cos(angles) + lower_half * jnp.sin(angles),
        ],
        axis=-1,
    )


def dispatch_table(expert_rows, experts, capacity):
    flat_ids = expert_rows.reshape(-1)
    hit_table = (flat_ids[:, None] == jnp.arange(experts, dtype=jnp.int32)[None, :]).astype(
        jnp.int32
    )
    slot_rank = jnp.sum((jnp.cumsum(hit_table, axis=0) - hit_table) * hit_table, axis=1)
    slot_index = flat_ids * capacity + slot_rank
    picked = (
        slot_index[None, :] == jnp.arange(experts * capacity, dtype=jnp.int32)[:, None]
    ).astype(jnp.float32)
    return picked.reshape(experts * capacity, expert_rows.shape[0], expert_rows.shape[1])


def route_weights(expert_in, group_router, expert_router, expert_ids, per_group):
    group_logits = jnp.dot(expert_in, group_router, preferred_element_type=jnp.float32)
    expert_logits = jnp.dot(expert_in, expert_router, preferred_element_type=jnp.float32)
    chosen = expert_ids[:, 0] // per_group
    group_hit = (
        jnp.arange(group_logits.shape[1], dtype=jnp.int32)[None, :] == chosen[:, None]
    ).astype(jnp.float32)
    chosen_logit = jnp.sum(group_logits * group_hit, axis=1, keepdims=True)
    group_share = 1.0 / jnp.sum(jnp.exp(group_logits - chosen_logit), axis=1)
    expert_hit = (
        expert_ids[:, :, None] == jnp.arange(expert_logits.shape[1], dtype=jnp.int32)[None, None, :]
    ).astype(jnp.float32)
    picked_logit = jnp.sum(expert_hit * expert_logits[:, None, :], axis=2)
    inner_share = 1.0 / jnp.sum(
        jnp.exp(picked_logit[:, None, :] - picked_logit[:, :, None]), axis=2
    )
    return group_share[:, None] * inner_share


def on_device(
    residual,
    cache_latent,
    cache_rope,
    lengths,
    query_latent,
    query_rope,
    norm_gain,
    latent_weight,
    latent_gain,
    rope_weight,
    value_weight,
    out_weight,
    mixer_gain,
    group_router,
    expert_router,
    expert_ids,
    gate_weight,
    up_weight,
    down_weight,
):
    ep_count = lax.axis_size("ep")
    seq_count = cache_latent.shape[0]
    group_rows = residual.shape[0]
    model_width = residual.shape[1]
    resid_f = residual.astype(jnp.float32)
    own_rows = lax.dynamic_slice_in_dim(resid_f, lax.axis_index("tp") * seq_count, seq_count, 0)
    normed = (own_rows * inverse_rms(own_rows) * norm_gain.astype(jnp.float32)).astype(jnp.bfloat16)
    latent_raw = jnp.dot(normed, latent_weight, preferred_element_type=jnp.float32)
    new_latent = (latent_raw * inverse_rms(latent_raw) * latent_gain.astype(jnp.float32)).astype(
        jnp.bfloat16
    )
    positions = lengths.astype(jnp.float32)
    rope_raw = jnp.dot(normed, rope_weight.T, preferred_element_type=jnp.float32)
    new_rope_key = rotate(rope_raw, positions).astype(jnp.bfloat16)
    query_turned = rotate(query_rope.astype(jnp.float32), positions[:, None]).astype(jnp.bfloat16)
    score_scale = (NOPE + ROPE) ** (-0.5)
    cached = (
        jnp.einsum("shc,spc->shp", query_latent, cache_latent, preferred_element_type=jnp.float32)
        + jnp.einsum("shr,srp->shp", query_turned, cache_rope, preferred_element_type=jnp.float32)
    ) * score_scale
    keeping = (
        jnp.arange(cache_latent.shape[1], dtype=jnp.int32)[None, None, :] < lengths[:, None, None]
    )
    cached = jnp.where(keeping, cached, -jnp.inf)
    fresh = (
        jnp.einsum("shc,sc->sh", query_latent, new_latent, preferred_element_type=jnp.float32)
        + jnp.einsum("shr,sr->sh", query_turned, new_rope_key, preferred_element_type=jnp.float32)
    ) * score_scale
    row_top = jnp.maximum(jnp.max(cached, axis=2), fresh)
    cached_exp = jnp.exp(cached - row_top[:, :, None])
    fresh_exp = jnp.exp(fresh - row_top)
    denominator = jnp.sum(cached_exp, axis=2) + fresh_exp
    cached_weight = (cached_exp / denominator[:, :, None]).astype(jnp.bfloat16)
    fresh_weight = (fresh_exp / denominator).astype(jnp.bfloat16)
    mixed_latent = (
        jnp.einsum("shp,spc->shc", cached_weight, cache_latent, preferred_element_type=jnp.float32)
        + fresh_weight.astype(jnp.float32)[:, :, None] * new_latent.astype(jnp.float32)[:, None, :]
    ).astype(jnp.bfloat16)
    head_values = jnp.einsum(
        "shc,chv->shv",
        mixed_latent,
        value_weight.reshape(KV, H, V),
        preferred_element_type=jnp.float32,
    ).astype(jnp.bfloat16)
    by_heads = lax.all_to_all(head_values, "tp", split_axis=1, concat_axis=0, tiled=True)
    head_terms = jnp.dot(
        by_heads.reshape(group_rows, -1), out_weight, preferred_element_type=jnp.float32
    )
    attended = lax.psum(head_terms, "tp")
    after_attention = (resid_f + attended).astype(jnp.bfloat16)
    after_f = after_attention.astype(jnp.float32)
    expert_in = (after_f * inverse_rms(after_f) * mixer_gain.astype(jnp.float32)).astype(
        jnp.bfloat16
    )
    experts = expert_router.shape[1]
    capacity = 2 * group_rows * TOPK // experts
    route_weight = route_weights(
        expert_in, group_router, expert_router, expert_ids, experts // GROUPS
    )
    picked = dispatch_table(expert_ids, experts, capacity)
    select_rows = jnp.sum(picked, axis=2).astype(jnp.bfloat16)
    outbound = jnp.dot(select_rows, expert_in, preferred_element_type=jnp.float32).astype(
        jnp.bfloat16
    )
    outbound = outbound.reshape(ep_count, gate_weight.shape[0], capacity, model_width)
    rows = lax.all_to_all(outbound, "ep", split_axis=0, concat_axis=0, tiled=True)
    gate_value = jnp.einsum("secd,edf->secf", rows, gate_weight, preferred_element_type=jnp.float32)
    up_value = jnp.einsum("secd,edf->secf", rows, up_weight, preferred_element_type=jnp.float32)
    activation = (jax.nn.silu(gate_value) * up_value).astype(jnp.bfloat16)
    expert_terms = jnp.einsum(
        "secf,efd->secd", activation, down_weight, preferred_element_type=jnp.float32
    )
    combine = jnp.sum(picked * route_weight[None, :, :], axis=2).T
    summed_terms = lax.psum_scatter(expert_terms, "tp", scatter_dimension=3, tiled=True)
    returned_terms = lax.all_to_all(summed_terms, "ep", split_axis=0, concat_axis=0, tiled=True)
    share_width = returned_terms.shape[3]
    moe_part = jnp.dot(
        combine, returned_terms.reshape(-1, share_width), precision=lax.Precision.HIGHEST
    )
    after_cols = lax.dynamic_slice_in_dim(
        after_f, lax.axis_index("tp") * share_width, share_width, 1
    )
    mixed_share = (after_cols + moe_part).astype(jnp.bfloat16)
    mixed = lax.all_gather(mixed_share, "tp", axis=1, tiled=True)
    return (mixed, new_latent, new_rope_key)


def solution(mesh):
    in_specs = (
        P("ep", None),
        P(("ep", "tp"), None, None),
        P(("ep", "tp"), None, None),
        P(("ep", "tp")),
        P(("ep", "tp"), None, None),
        P(("ep", "tp"), None, None),
        P(),
        P(),
        P(),
        P(),
        P(),
        P("tp", None),
        P(),
        P(),
        P(),
        P("ep", None),
        P("ep", None, "tp"),
        P("ep", None, "tp"),
        P("ep", "tp", None),
    )
    out_specs = (P("ep", None), P(("ep", "tp"), None), P(("ep", "tp"), None))
    return jax.shard_map(
        on_device, mesh=mesh, in_specs=in_specs, out_specs=out_specs, check_vma=False
    )
```

profile of v0, /device:TPU:0, one launch (start us, length us, event | category | flops | bytes accessed | tf_op | source)
XLA Modules:
  0.0 177.1 jit_solution(6395437696958432695)
XLA Ops:
  7.2 0.8 convert_element_type.79
  8.0 0.7 iota_compare_fusion.2
  8.7 0.9 convert_element_type.77
  9.8 0.7 convert_element_type.80
  10.5 0.8 convert_element_type.78
  11.3 1.1 fusion.50
  12.4 1.6 multiply_reduce_fusion.2
  14.7 3.5 %fusion.58 = f32[4,32,2048]{2,1,0:T(8,128)S(1)} fusion(bf16[4,32,256]{2,1,0:T(8,128)(2,1)} %param.23, bf16[4,2048,256]{2,1,0:T(8,128)(2,1)} %param.20), kind=kOutput, calls=%fused_computation.90 | convolution fusion | flops 134217728 | bytes 5308416 | tf_op jit(solution)/shard_map/shc,spc->shp/dot_general | solution.py:108
  19.8 1.5 copy.61
  21.3 3.1 %fusion.23 = bf16[4,32,256]{2,1,0:T(8,128)(2,1)S(1)} fusion(bf16[4,2048,256]{2,1,0:T(8,128)(2,1)} %param.20, f32[4,32,2048]{2,1,0:T(8,128)S(1)} %get-tuple-element.18, f32[4,32]{1,0:T(4,128)S(1)} %get-tuple-element.12, f32[4,32]{1,0:T(4,128)S(1)} %fusion.44, f32[4,256]{1,0:T(4,128)S(1)} %get-tuple-element.7, f32[4,32]{1,0:T(4,128)S(1)} %get-tuple-element.11), kind=kOutput, calls=%fused_computation.16 | convolution fusion | flops 135102464 | bytes 5314048 | tf_op jit(solution)/shard_map/shp,spc->shc/dot_general | solution.py:126
  24.8 0.7 reshape.194
  25.5 6.4 %all-to-all-start = ((bf16[8,2,512]{2,1,0:T(2,128)(2,1)}), bf16[8,2,512]{2,1,0:T(2,128)(2,1)S(1)}, u32[]{:S(2)}, u32[]{:S(2)}) async-start(bf16[8,2,512]{2,1,0:T(2,128)(2,1)} %reshape.194), calls=%async_computation | async-start | bytes 32768 | tf_op jit(solution)/shard_map/all_to_all | solution.py:135
  32.7 4.8 %all-to-all-done = bf16[8,2,512]{2,1,0:T(2,128)(2,1)S(1)} async-done(((bf16[8,2,512]{2,1,0:T(2,128)(2,1)}), bf16[8,2,512]{2,1,0:T(2,128)(2,1)S(1)}, u32[]{:S(2)}, u32[]{:S(2)}) %all-to-all-start) | async-done | bytes 16416 | tf_op jit(solution)/shard_map/all_to_all | solution.py:135
  37.7 1.0 fusion.59
  38.8 53.8 %all-reduce.2.cloned.1.call-done = f32[32,2048]{1,0:T(8,128)} async-done(((f32[32,2048]{1,0:T(8,128)}), f32[32,2048]{1,0:T(8,128)}) %all-reduce.2.cloned.1.call-update) | async-done | bytes 262160 | tf_op jit(solution)/shard_map/psum | solution.py:139
  92.6 1.1 multiply_reduce_fusion
  94.6 10.6 %all_to_all.25 = bf16[4,2,16,2048]{3,2,1,0:T(8,128)(2,1)S(1)} all-to-all(bf16[4,2,16,2048]{3,2,1,0:T(8,128)(2,1)S(1)} %bitcast.81), channel_id=1, replica_groups=mesh['ep'=4,'tp'=8] {'ep'}, dimensions={0} | all-to-all | bytes 1048576 | tf_op jit(solution)/shard_map/all_to_all | solution.py:156
  105.2 3.0 %fusion.11 = f32[4,2,16,512]{3,2,0,1:T(8,128)S(1)} fusion(bf16[2,2048,512]{2,1,0:T(8,128)(2,1)} %param.35, bf16[4,2,16,2048]{3,2,1,0:T(8,128)(2,1)S(1)} %all_to_all.25), kind=kOutput, calls=%fused_computation.11 | convolution fusion | flops 268435456 | bytes 4980736 | tf_op jit(solution)/shard_map/secd,edf->secf/dot_general | solution.py:157
  108.2 6.0 %fusion.6 = f32[4,2,16,2048]{3,2,0,1:T(8,128)} fusion(bf16[2,512,2048]{2,1,0:T(8,128)(2,1)} %param.37, bf16[2,2048,512]{2,1,0:T(8,128)(2,1)} %param.36, bf16[4,2,16,2048]{3,2,1,0:T(8,128)(2,1)S(1)} %all_to_all.25, f32[4,2,16,512]{3,2,0,1:T(8,128)S(1)} %fusion.11), kind=kOutput, calls=%fused_computation.6 | convolution fusion | flops 537264128 | bytes 10223616 | tf_op jit(solution)/shard_map/secf,efd->secd/dot_general | solution.py:160
  114.3 30.9 %reduce-scatter.2.cloned.1.call-done = f32[4,2,16,256]{3,2,0,1:T(8,128)} async-done(((f32[4,2,16,2048]{3,2,0,1:T(8,128)}), f32[4,2,16,256]{3,2,0,1:T(8,128)}) %reduce-scatter.2.cloned.1.call-update) | async-done | bytes 131088 | tf_op jit(solution)/shard_map/reduce_scatter | solution.py:164
  145.2 1.6 copy.68
  146.8 3.7 %all-to-all-start.2 = ((f32[4,2,16,256]{3,2,1,0:T(8,128)}), f32[4,2,16,256]{3,2,1,0:T(8,128)S(1)}, u32[]{:S(2)}, u32[]{:S(2)}) async-start(f32[4,2,16,256]{3,2,1,0:T(8,128)} %copy.68), calls=%async_computation.3 | async-start | bytes 262144 | tf_op jit(solution)/shard_map/all_to_all | solution.py:165
  151.1 4.4 %all-to-all-done.2 = f32[4,2,16,256]{3,2,1,0:T(8,128)S(1)} async-done(((f32[4,2,16,256]{3,2,1,0:T(8,128)}), f32[4,2,16,256]{3,2,1,0:T(8,128)S(1)}, u32[]{:S(2)}, u32[]{:S(2)}) %all-to-all-start.2) | async-done | bytes 131104 | tf_op jit(solution)/shard_map/all_to_all | solution.py:165
  155.6 14.0 %all_gather.3 = bf16[32,2048]{1,0:T(8,128)(2,1)S(1)} all-gather(bf16[32,256]{1,0:T(8,128)(2,1)S(1)} %fusion.25), channel_id=1, replica_groups=mesh['ep'=4,'tp'=8] {'tp'}, dimensions={1}, use_global_device_ids=true | all-gather | bytes 147456 | tf_op jit(solution)/shard_map/all_gather | solution.py:174
  (65 shorter events, 6.2 us)
Async XLA Ops:
  7.2 30.6 %copy-start = (bf16[256,2048]{1,0:T(8,128)(2,1)S(1)}, bf16[256,2048]{1,0:T(8,128)(2,1)}, u32[]{:S(2)}) copy-start(bf16[256,2048]{1,0:T(8,128)(2,1)} %param.30) | copy-start | bytes 3145732
  7.2 11.1 %copy-start.3 = (bf16[4,32,256]{2,1,0:T(8,128)(2,1)S(1)}, bf16[4,32,256]{2,1,0:T(8,128)(2,1)}, u32[]{:S(2)}) copy-start(bf16[4,32,256]{2,1,0:T(8,128)(2,1)} %param.23) | copy-start | bytes 196612
  7.2 11.7 %copy-start.2 = (bf16[4,32,2048]{2,1,0:T(8,128)(2,1)S(1)}, bf16[4,32,2048]{2,1,0:T(8,128)(2,1)}, u32[]{:S(2)}) copy-start(bf16[4,32,2048]{2,1,0:T(8,128)(2,1)} %param.21) | copy-start | bytes 1572868
  18.3 6.1 %copy-start.7 = (bf16[4,256]{1,0:T(4,128)(2,1)}, bf16[4,256]{1,0:T(4,128)(2,1)S(1)}, u32[]{:S(2)}) copy-start(bf16[4,256]{1,0:T(4,128)(2,1)S(1)} %get-tuple-element.27) | copy-start | bytes 6148
  21.2 10.7 %copy-start.5 = (s32[32,2]{0,1:T(2,128)S(1)}, s32[32,2]{0,1:T(2,128)}, u32[]{:S(2)}) copy-start(s32[32,2]{0,1:T(2,128)} %param.34) | copy-start | bytes 772
  21.3 11.4 %copy-start.6 = (bf16[2048]{0:T(1024)(128)(2,1)S(1)}, bf16[2048]{0:T(1024)(128)(2,1)}, u32[]{:S(2)}) copy-start(bf16[2048]{0:T(1024)(128)(2,1)} %param.31) | copy-start | bytes 12292
  21.3 71.3 %copy-start.1 = (bf16[32,2048]{1,0:T(8,128)(2,1)S(1)}, bf16[32,2048]{1,0:T(8,128)(2,1)}, u32[]{:S(2)}) copy-start(bf16[32,2048]{1,0:T(8,128)(2,1)} %param.19) | copy-start | bytes 393220
  21.3 72.5 %copy-start.8 = (bf16[2048,4]{0,1:T(4,128)(2,1)S(1)}, bf16[2048,4]{0,1:T(4,128)(2,1)}, u32[]{:S(2)}) copy-start(bf16[2048,4]{0,1:T(4,128)(2,1)} %param.32) | copy-start | bytes 49156
  21.3 72.7 %copy-start.4 = (bf16[2048,8]{0,1:T(8,128)(2,1)S(1)}, bf16[2048,8]{0,1:T(8,128)(2,1)}, u32[]{:S(2)}) copy-start(bf16[2048,8]{0,1:T(8,128)(2,1)} %param.33) | copy-start | bytes 98308
  25.5 12.0 %all-to-all-start = ((bf16[8,2,512]{2,1,0:T(2,128)(2,1)}), bf16[8,2,512]{2,1,0:T(2,128)(2,1)S(1)}, u32[]{:S(2)}, u32[]{:S(2)}) async-start(bf16[8,2,512]{2,1,0:T(2,128)(2,1)} %reshape.194), calls=%async_computation | async-start | bytes 32768 | tf_op jit(solution)/shard_map/all_to_all | solution.py:135
  31.9 60.7 %all-reduce.2.cloned.1.call-start = ((), (), s32[]{:S(2)}) async-start(), calls=%async_computation.4 | async-start | bytes 524288 | tf_op jit(solution)/shard_map/psum | solution.py:139
  38.7 106.5 %reduce-scatter.2.cloned.1.call-start = ((), (), s32[]{:S(2)}) async-start(), calls=%async_computation.5 | async-start | bytes 1179648 | tf_op jit(solution)/shard_map/reduce_scatter | solution.py:164
  146.8 8.7 %all-to-all-start.2 = ((f32[4,2,16,256]{3,2,1,0:T(8,128)}), f32[4,2,16,256]{3,2,1,0:T(8,128)S(1)}, u32[]{:S(2)}, u32[]{:S(2)}) async-start(f32[4,2,16,256]{3,2,1,0:T(8,128)} %copy.68), calls=%async_computation.3 | async-start | bytes 262144 | tf_op jit(solution)/shard_map/all_to_all | solution.py:165
Sparse Core Ops, SparseCore 0:
  38.9 53.6 all-reduce.1
  114.4 30.7 reduce-scatter.1
where the time goes:
time: 178 us; the launch traced here: 177 us
  waiting for transfers between devices  93.9 us (53%)
  blocking collectives  24.5 us (14%)
  matrix products  21.4 us (12%)
  between operations  14.3 us (8%)
  starting transfers between devices  10.1 us (6%)
  other arithmetic  7.81 us (4%)
  local copies, waits for them, and re-layouts  5.06 us (3%)
    psum x1, waiting for transfers between devices, on_device(): attended = lax.psum(head_terms, 'tp')  53.8 us
    reduce_scatter x1, waiting for transfers between devices, on_device(): lax.psum_scatter(expert_terms, 'tp', scatter_dimension=3, tiled=True)  30.9 us
    all_gather x1, blocking collectives, on_device(): mixed = lax.all_gather(mixed_share, 'tp', axis=1, tiled=True)  14 us
    all_to_all x1, blocking collectives, on_device(): lax.all_to_all(outbound, 'ep', split_axis=0, concat_axis=0, tiled=True)  10.6 us
    all_to_all x1, starting transfers between devices, on_device(): lax.all_to_all(head_values, 'tp', split_axis=1, concat_axis=0, tiled=True)  6.35 us
    dot_general x1, matrix products, on_device(): jnp.einsum('secf,efd->secd', activation, down_weight, preferred_element_t...  6.04 us
    all_to_all x1, waiting for transfers between devices, on_device(): lax.all_to_all(head_values, 'tp', split_axis=1, concat_axis=0, tiled=True)  4.83 us
    all_to_all x1, waiting for transfers between devices, on_device(): lax.all_to_all(summed_terms, 'ep', split_axis=0, concat_axis=0, tiled=True)  4.38 us
  transfers between devices with their start and end apart: 4, of which 4 were waited for; matrix products, arithmetic and copies ran while one was open for 1% of the time, Pallas kernels for 0%

commit v1 on v0

--- a/solution.py
+++ b/solution.py
@@ -136,7 +136,9 @@
     head_terms = jnp.dot(
         by_heads.reshape(group_rows, -1), out_weight, preferred_element_type=jnp.float32
     )
-    attended = lax.psum(head_terms, "tp")
+    attended = head_terms
+    for hop in (1, 2, 4):
+        attended = attended + lax.ppermute(attended, "tp", [(dev, dev ^ hop) for dev in range(8)])
     after_attention = (resid_f + attended).astype(jnp.bfloat16)
     after_f = after_attention.astype(jnp.float32)
     expert_in = (after_f * inverse_rms(after_f) * mixer_gain.astype(jnp.float32)).astype(

time: 178 us -> 146 us (0.82)
  waiting for transfers between devices: 93.9 us -> 55.8 us
  blocking collectives: 24.5 us -> 37.9 us
  starting transfers between devices: 10.1 us -> 5.08 us
    psum x1 -> x0, waiting for transfers between devices: 53.8 us -> none  [on_device(): attended = lax.psum(head_terms, 'tp')]
    ppermute x0 -> x3, waiting for transfers between devices: none -> 22 us  [on_device(): lax.ppermute(attended, 'tp', [(dev, dev ^ hop) for dev in range(8)])]
    all_to_all x0 -> x1, blocking collectives: none -> 11.8 us  [on_device(): lax.all_to_all(head_values, 'tp', split_axis=1, concat_axis=0, tiled=True)]
    all_to_all x1 -> x0, starting transfers between devices: 6.35 us -> none  [on_device(): lax.all_to_all(head_values, 'tp', split_axis=1, concat_axis=0, tiled=True)]
    all_to_all x1 -> x0, waiting for transfers between devices: 4.83 us -> none  [on_device(): lax.all_to_all(head_values, 'tp', split_axis=1, concat_axis=0, tiled=True)]
  transfers between devices with their start and end apart: 4 -> 5, of which waited for: 4 -> 5; matrix products, arithmetic and copies ran while one was open for 1% -> 1% of each run, Pallas kernels for 0% -> 0%
where the time goes in v1:
time: 146 us; the launch traced here: 145 us
  waiting for transfers between devices  55.8 us (38%)
  blocking collectives  37.9 us (26%)
  matrix products  20.6 us (14%)
  between operations  14.3 us (10%)
  other arithmetic  6.9 us (5%)
  starting transfers between devices  5.08 us (3%)
  local copies, waits for them, and re-layouts  4.44 us (3%)
    reduce_scatter x1, waiting for transfers between devices, on_device(): lax.psum_scatter(expert_terms, 'tp', scatter_dimension=3, tiled=True)  29.4 us
    ppermute x3, waiting for transfers between devices, on_device(): lax.ppermute(attended, 'tp', [(dev, dev ^ hop) for dev in range(8)])  22 us
    all_gather x1, blocking collectives, on_device(): mixed = lax.all_gather(mixed_share, 'tp', axis=1, tiled=True)  14 us
    all_to_all x1, blocking collectives, on_device(): lax.all_to_all(outbound, 'ep', split_axis=0, concat_axis=0, tiled=True)  12.2 us
    all_to_all x1, blocking collectives, on_device(): lax.all_to_all(head_values, 'tp', split_axis=1, concat_axis=0, tiled=True)  11.8 us
    dot_general x1, matrix products, on_device(): jnp.einsum('secf,efd->secd', activation, down_weight, preferred_element_t...  6.04 us
    all_to_all x1, waiting for transfers between devices, on_device(): lax.all_to_all(summed_terms, 'ep', split_axis=0, concat_axis=0, tiled=True)  4.38 us
    all_to_all x1, starting transfers between devices, on_device(): lax.all_to_all(summed_terms, 'ep', split_axis=0, concat_axis=0, tiled=True)  3.72 us
  transfers between devices with their start and end apart: 5, of which 5 were waited for; matrix products, arithmetic and copies ran while one was open for 1% of the time, Pallas kernels for 0%

profile of v1, /device:TPU:0, one launch (start us, length us, event | category | flops | bytes accessed | tf_op | source)
XLA Modules:
  0.0 145.1 jit_solution(1161917468706852740)
XLA Ops:
  7.3 0.8 convert_element_type.79
  8.0 0.7 iota_compare_fusion.2
  8.8 0.9 convert_element_type.77
  9.9 0.7 convert_element_type.80
  10.5 0.8 convert_element_type.78
  11.3 1.1 fusion.49
  12.4 1.6 %multiply_reduce_fusion.2 = (f32[4]{0:T(128)S(1)}, f32[4,256]{1,0:T(4,128)S(1)}) fusion(bf16[2048,256]{1,0:T(8,128)(2,1)} %param.26, f32[32,2048]{1,0:T(8,128)S(1)} %convert_element_type.77, s32[]{:T(128)S(6)} %select_n.17, f32[2048]{0:T(1024)S(1)} %convert_element_type.80, f32[4]{0:T(128)S(1)} %add_rsqrt_fusion.2), kind=kOutput, calls=%fused_computation.52 | convolution fusion | flops 4220924 | bytes 1094164 | tf_op jit(solution)/shard_map/dot_general | solution.py:98
  14.1 0.7 convert_element_type.82
  14.7 3.5 %fusion.57 = f32[4,32,2048]{2,1,0:T(8,128)S(1)} fusion(bf16[4,32,256]{2,1,0:T(8,128)(2,1)} %param.23, bf16[4,2048,256]{2,1,0:T(8,128)(2,1)} %param.20), kind=kOutput, calls=%fused_computation.89 | convolution fusion | flops 134217728 | bytes 5308416 | tf_op jit(solution)/shard_map/shc,spc->shp/dot_general | solution.py:108
  19.8 1.5 %copy.61 = bf16[256,2048]{0,1:T(8,128)(2,1)S(1)} copy(bf16[256,2048]{1,0:T(8,128)(2,1)} %param.29) | data formatting | bytes 2097152 | tf_op args[10]
  21.3 3.0 %fusion.23 = bf16[4,32,256]{2,1,0:T(8,128)(2,1)S(1)} fusion(bf16[4,2048,256]{2,1,0:T(8,128)(2,1)} %param.20, f32[4,32,2048]{2,1,0:T(8,128)S(1)} %get-tuple-element.18, f32[4,32]{1,0:T(4,128)S(1)} %get-tuple-element.12, f32[4,32]{1,0:T(4,128)S(1)} %fusion.43, f32[4,256]{1,0:T(4,128)S(1)} %get-tuple-element.7, f32[4,32]{1,0:T(4,128)S(1)} %get-tuple-element.11), kind=kOutput, calls=%fused_computation.16 | convolution fusion | flops 135102464 | bytes 5314048 | tf_op jit(solution)/shard_map/shp,spc->shc/dot_general | solution.py:126
  24.9 11.8 %all_to_all.25 = bf16[8,2,512]{2,1,0:T(2,128)(2,1)S(1)} all-to-all(bf16[8,2,512]{2,1,0:T(2,128)(2,1)S(1)} %reshape.194), channel_id=1, replica_groups=mesh['ep'=4,'tp'=8] {'tp'}, dimensions={0} | all-to-all | bytes 32768 | tf_op jit(solution)/shard_map/all_to_all | solution.py:135
  37.5 1.3 collective-permute-done
  38.8 0.7 collective-permute-start.1
  39.7 7.6 %collective-permute-done.1 = f32[32,2048]{1,0:T(8,128)S(1)} collective-permute-done((f32[32,2048]{1,0:T(8,128)S(1)}, f32[32,2048]{1,0:T(8,128)S(1)}, u32[]{:S(2)}, u32[]{:S(2)}) %collective-permute-start.1) | collective-permute-done | bytes 262176 | tf_op jit(solution)/shard_map/ppermute | solution.py:141
  48.3 13.1 %collective-permute-done.2 = f32[32,2048]{1,0:T(8,128)S(1)} collective-permute-done((f32[32,2048]{1,0:T(8,128)S(1)}, f32[32,2048]{1,0:T(8,128)S(1)}, u32[]{:S(2)}, u32[]{:S(2)}) %collective-permute-start.2) | collective-permute-done | bytes 262176 | tf_op jit(solution)/shard_map/ppermute | solution.py:141
  62.5 12.2 %all_to_all.26 = bf16[4,2,16,2048]{3,2,1,0:T(8,128)(2,1)S(1)} all-to-all(bf16[4,2,16,2048]{3,2,1,0:T(8,128)(2,1)S(1)} %bitcast.81), channel_id=1, replica_groups=mesh['ep'=4,'tp'=8] {'ep'}, dimensions={0} | all-to-all | bytes 1048576 | tf_op jit(solution)/shard_map/all_to_all | solution.py:158
  74.6 3.0 %fusion.11 = f32[4,2,16,512]{3,2,0,1:T(8,128)S(1)} fusion(bf16[2,2048,512]{2,1,0:T(8,128)(2,1)} %param.35, bf16[4,2,16,2048]{3,2,1,0:T(8,128)(2,1)S(1)} %all_to_all.26), kind=kOutput, calls=%fused_computation.11 | convolution fusion | flops 268435456 | bytes 4980736 | tf_op jit(solution)/shard_map/secd,edf->secf/dot_general | solution.py:159
  77.7 6.0 %fusion.6 = f32[4,2,16,2048]{3,2,0,1:T(8,128)} fusion(bf16[2,512,2048]{2,1,0:T(8,128)(2,1)} %param.37, bf16[2,2048,512]{2,1,0:T(8,128)(2,1)} %param.36, bf16[4,2,16,2048]{3,2,1,0:T(8,128)(2,1)S(1)} %all_to_all.26, f32[4,2,16,512]{3,2,0,1:T(8,128)S(1)} %fusion.11), kind=kOutput, calls=%fused_computation.6 | convolution fusion | flops 537264128 | bytes 10223616 | tf_op jit(solution)/shard_map/secf,efd->secd/dot_general | solution.py:162
  83.7 29.4 %reduce-scatter.2.cloned.1.call-done = f32[4,2,16,256]{3,2,0,1:T(8,128)} async-done(((f32[4,2,16,2048]{3,2,0,1:T(8,128)}), f32[4,2,16,256]{3,2,0,1:T(8,128)}) %reduce-scatter.2.cloned.1.call-update) | async-done | bytes 131088 | tf_op jit(solution)/shard_map/reduce_scatter | solution.py:166
  113.2 1.6 %copy.68 = f32[4,2,16,256]{3,2,1,0:T(8,128)} copy(f32[4,2,16,256]{3,2,0,1:T(8,128)} %reduce-scatter.2.cloned.1.call-done) | data formatting | bytes 262144 | tf_op jit(solution)/shard_map/reduce_scatter | solution.py:166
  114.7 3.7 %all-to-all-start.2 = ((f32[4,2,16,256]{3,2,1,0:T(8,128)}), f32[4,2,16,256]{3,2,1,0:T(8,128)S(1)}, u32[]{:S(2)}, u32[]{:S(2)}) async-start(f32[4,2,16,256]{3,2,1,0:T(8,128)} %copy.68), calls=%async_computation.3 | async-start | bytes 262144 | tf_op jit(solution)/shard_map/all_to_all | solution.py:167
  119.1 4.4 %all-to-all-done.2 = f32[4,2,16,256]{3,2,1,0:T(8,128)S(1)} async-done(((f32[4,2,16,256]{3,2,1,0:T(8,128)}), f32[4,2,16,256]{3,2,1,0:T(8,128)S(1)}, u32[]{:S(2)}, u32[]{:S(2)}) %all-to-all-start.2) | async-done | bytes 131104 | tf_op jit(solution)/shard_map/all_to_all | solution.py:167
  123.6 14.0 %all_gather.3 = bf16[32,2048]{1,0:T(8,128)(2,1)S(1)} all-gather(bf16[32,256]{1,0:T(8,128)(2,1)S(1)} %add_convert_fusion.2), channel_id=1, replica_groups=mesh['ep'=4,'tp'=8] {'tp'}, dimensions={1}, use_global_device_ids=true | all-gather | bytes 147456 | tf_op jit(solution)/shard_map/all_gather | solution.py:176
  (69 shorter events, 6.7 us)
Async XLA Ops:
  7.2 29.8 %copy-start = (bf16[256,2048]{1,0:T(8,128)(2,1)S(1)}, bf16[256,2048]{1,0:T(8,128)(2,1)}, u32[]{:S(2)}) copy-start(bf16[256,2048]{1,0:T(8,128)(2,1)} %param.30) | copy-start | bytes 3145732
  7.2 11.2 %copy-start.3 = (bf16[4,32,256]{2,1,0:T(8,128)(2,1)S(1)}, bf16[4,32,256]{2,1,0:T(8,128)(2,1)}, u32[]{:S(2)}) copy-start(bf16[4,32,256]{2,1,0:T(8,128)(2,1)} %param.23) | copy-start | bytes 196612
  7.2 11.8 %copy-start.2 = (bf16[4,32,2048]{2,1,0:T(8,128)(2,1)S(1)}, bf16[4,32,2048]{2,1,0:T(8,128)(2,1)}, u32[]{:S(2)}) copy-start(bf16[4,32,2048]{2,1,0:T(8,128)(2,1)} %param.21) | copy-start | bytes 1572868
  7.2 105.9 %reduce-scatter.2.cloned.1.call-start = ((), (), s32[]{:S(2)}) async-start(), calls=%async_computation.4 | async-start | bytes 1179648 | tf_op jit(solution)/shard_map/reduce_scatter | solution.py:166
  18.3 6.0 %copy-start.7 = (bf16[4,256]{1,0:T(4,128)(2,1)}, bf16[4,256]{1,0:T(4,128)(2,1)S(1)}, u32[]{:S(2)}) copy-start(bf16[4,256]{1,0:T(4,128)(2,1)S(1)} %get-tuple-element.27) | copy-start | bytes 6148
  21.3 16.0 %copy-start.5 = (s32[32,2]{0,1:T(2,128)S(1)}, s32[32,2]{0,1:T(2,128)}, u32[]{:S(2)}) copy-start(s32[32,2]{0,1:T(2,128)} %param.34) | copy-start | bytes 772
  21.3 26.8 %copy-start.6 = (bf16[2048]{0:T(1024)(128)(2,1)S(1)}, bf16[2048]{0:T(1024)(128)(2,1)}, u32[]{:S(2)}) copy-start(bf16[2048]{0:T(1024)(128)(2,1)} %param.31) | copy-start | bytes 12292
  21.3 40.0 %copy-start.1 = (bf16[32,2048]{1,0:T(8,128)(2,1)S(1)}, bf16[32,2048]{1,0:T(8,128)(2,1)}, u32[]{:S(2)}) copy-start(bf16[32,2048]{1,0:T(8,128)(2,1)} %param.19) | copy-start | bytes 393220
  24.4 37.2 %copy-start.8 = (bf16[2048,4]{0,1:T(4,128)(2,1)S(1)}, bf16[2048,4]{0,1:T(4,128)(2,1)}, u32[]{:S(2)}) copy-start(bf16[2048,4]{0,1:T(4,128)(2,1)} %param.32) | copy-start | bytes 49156
  24.4 37.4 %copy-start.4 = (bf16[2048,8]{0,1:T(8,128)(2,1)S(1)}, bf16[2048,8]{0,1:T(8,128)(2,1)}, u32[]{:S(2)}) copy-start(bf16[2048,8]{0,1:T(8,128)(2,1)} %param.33) | copy-start | bytes 98308
  37.2 1.6 %collective-permute-start = (f32[32,2048]{1,0:T(8,128)S(1)}, f32[32,2048]{1,0:T(8,128)S(1)}, u32[]{:S(2)}, u32[]{:S(2)}) collective-permute-start(f32[32,2048]{1,0:T(8,128)S(1)} %fusion.58), channel_id=1, source_target_pairs={{0,1},{1,0},{2,3},{3,2},{4,5},{5,4},{6,7},{7,6},{8,9},{9,8},{10,11... | collective-permute-start | bytes 786440 | tf_op jit(solution)/shard_map/ppermute | solution.py:141
  38.8 8.4 %collective-permute-start.1 = (f32[32,2048]{1,0:T(8,128)S(1)}, f32[32,2048]{1,0:T(8,128)S(1)}, u32[]{:S(2)}, u32[]{:S(2)}) collective-permute-start(f32[32,2048]{1,0:T(8,128)S(1)} %add.90), channel_id=1, source_target_pairs={{0,2},{1,3},{2,0},{3,1},{4,6},{5,7},{6,4},{7,5},{8,10},{9,11},{10,... | collective-permute-start | bytes 786440 | tf_op jit(solution)/shard_map/ppermute | solution.py:141
  47.3 14.1 %collective-permute-start.2 = (f32[32,2048]{1,0:T(8,128)S(1)}, f32[32,2048]{1,0:T(8,128)S(1)}, u32[]{:S(2)}, u32[]{:S(2)}) collective-permute-start(f32[32,2048]{1,0:T(8,128)S(1)} %add.91), channel_id=1, source_target_pairs={{0,4},{1,5},{2,6},{3,7},{4,0},{5,1},{6,2},{7,3},{8,12},{9,13},{10,... | collective-permute-start | bytes 786440 | tf_op jit(solution)/shard_map/ppermute | solution.py:141
  114.7 8.7 %all-to-all-start.2 = ((f32[4,2,16,256]{3,2,1,0:T(8,128)}), f32[4,2,16,256]{3,2,1,0:T(8,128)S(1)}, u32[]{:S(2)}, u32[]{:S(2)}) async-start(f32[4,2,16,256]{3,2,1,0:T(8,128)} %copy.68), calls=%async_computation.3 | async-start | bytes 262144 | tf_op jit(solution)/shard_map/all_to_all | solution.py:167
Sparse Core Ops, SparseCore 0:
  83.9 29.2 reduce-scatter.1
